TPU v7x, 32 devices: a whole 2x2x4 slice. The times are simulated.
32 devices in a mesh: kv: 8 (over z, y), tp: 4 (over x, core).
Axes of the slice: x: 2, y: 2, z: 4, core: 2. Of those that a mesh axis runs over, the one named last changes fastest.
Arguments:
- queries: bfloat16 [6144, 2048], P('kv', 'tp'), may hold values from -6 to 6
- keys_values: bfloat16 [6144, 1024], P('kv', 'tp'), may hold values from -6 to 6
- log_sums: float32 [6144, 32], P('kv', 'tp'), may hold values from 6.5 to 7.5
- out_grad: bfloat16 [6144, 2048], P('kv', 'tp'), may hold values from -96 to 96
- inputs: bfloat16 [6144, 4096], P('kv'), may hold values from -0.046875 to 0.046875
- chosen: int32 [48, 16], P('kv'), may hold values from -1 to 95, as said below
Outputs:
- query_grad: bfloat16 [6144, 2048], P('kv', 'tp')
- kv_grad: float32 [6144, 1024], P('kv', 'tp')
- weight_grad: float32 [4096, 2048], P('kv', 'tp')
Inputs may be any that keep to these rules, and one draw needn't show every extreme that they name: `chosen`: each row names distinct key blocks, none starting after the last position of that row's query block, and -1 in unused entries; at least half of 16 blocks are named where that many are allowed. From the query blocks of one index of kv, at most 6 distinct blocks of the 768 positions of any one index are named, and this most is reached on every index.
All inputs are finite; a program needn't handle non-finite values.
Results may differ from a plain program's by a relative error of at most 0.0051.
Values may be sent and summed in bfloat16 or wider, within the bound.
A program may use at most 128 MiB of HBM per device.

v0:
```python
import jax
import jax.numpy as jnp
from jax import lax
from jax.sharding import PartitionSpec as P

DH = 64
BLK = 64
QB = 128
NSEL = 16


def shards(queries, keys_values, log_sums, out_grad, inputs, chosen):
    score_scale = DH ** (-0.5)
    tok_count = queries.shape[0]
    heads_here = queries.shape[1] // DH
    kv_heads = keys_values.shape[1] // (2 * DH)
    group_size = heads_here // kv_heads
    row_width = keys_values.shape[1]
    blocks_here = tok_count // BLK
    query_blocks = tok_count // QB
    kv_count = lax.axis_size("kv")
    first_block = lax.axis_index("kv") * query_blocks
    capacity = blocks_here // 2
    total_blocks = kv_count * blocks_here
    flat_ids = chosen.reshape(-1)
    needed = jnp.any(
        flat_ids[:, None] == jnp.arange(total_blocks, dtype=jnp.int32)[None, :], axis=0
    )
    needed = needed.reshape(kv_count, blocks_here).astype(jnp.int32)
    rank_in = jnp.cumsum(needed, axis=1) - 1
    matches = (needed[:, :, None] == 1) & (
        rank_in[:, :, None] == jnp.arange(capacity, dtype=jnp.int32)[None, None, :]
    )
    request = jnp.sum(
        matches.astype(jnp.int32) * jnp.arange(blocks_here, dtype=jnp.int32)[None, :, None], axis=1
    )
    request = jnp.where(jnp.any(matches, axis=1), request, -1)
    slot_flat = (jnp.arange(kv_count, dtype=jnp.int32)[:, None] * capacity + rank_in).reshape(-1)
    slot_ids = jnp.where(chosen >= 0, slot_flat[jnp.maximum(chosen, 0)], 0)
    asked_ids = lax.all_to_all(request, "kv", split_axis=0, concat_axis=0, tiled=True)
    local_blocks = keys_values.reshape(blocks_here, BLK, row_width)
    fetched = local_blocks[jnp.maximum(asked_ids, 0)]
    key_table = lax.all_to_all(fetched, "kv", split_axis=0, concat_axis=0, tiled=True).reshape(
        kv_count * capacity, BLK, row_width
    )

    def one_block(grad_table, packed):
        query_rows, grad_rows, sum_rows, chosen_row, slot_row, offset = packed
        query_blk = query_rows.reshape(QB, kv_heads, group_size, DH)
        grad_blk = grad_rows.reshape(QB, kv_heads, group_size, DH)
        sums_blk = sum_rows.reshape(QB, kv_heads, group_size)
        picked = key_table[slot_row].reshape(NSEL * BLK, kv_heads, 2, DH)
        key_blk = picked[:, :, 0, :]
        value_blk = picked[:, :, 1, :]
        present = chosen_row >= 0
        key_pos = (
            jnp.maximum(chosen_row, 0)[:, None] * BLK + jnp.arange(BLK, dtype=jnp.int32)[None, :]
        ).reshape(-1)
        key_live = jnp.repeat(present, BLK)
        query_pos = (first_block + offset) * QB + jnp.arange(QB, dtype=jnp.int32)
        visible = key_live[None, :] & (key_pos[None, :] <= query_pos[:, None])
        scores = (
            jnp.einsum("qhgd,nhd->qhgn", query_blk, key_blk, preferred_element_type=jnp.float32)
            * score_scale
        )
        attn_prob = jnp.where(
            visible[:, None, None, :], jnp.exp(scores - sums_blk[..., None]), jnp.float32(0.0)
        )
        prob_round = attn_prob.astype(jnp.bfloat16)
        output = jnp.einsum(
            "qhgn,nhd->qhgd", prob_round, value_blk, preferred_element_type=jnp.float32
        )
        delta_row = jnp.sum(grad_blk * output, axis=-1)
        prob_grad = jnp.einsum(
            "qhgd,nhd->qhgn", grad_blk, value_blk, preferred_element_type=jnp.float32
        )
        score_round = (attn_prob * (prob_grad - delta_row[..., None])).astype(jnp.bfloat16)
        query_part = (
            score_scale
            * jnp.einsum("qhgn,nhd->qhgd", score_round, key_blk, preferred_element_type=jnp.float32)
        ).astype(jnp.bfloat16)
        key_part = score_scale * jnp.einsum(
            "qhgn,qhgd->nhd", score_round, query_blk, preferred_element_type=jnp.float32
        )
        value_part = jnp.einsum(
            "qhgn,qhgd->nhd", prob_round, grad_blk, preferred_element_type=jnp.float32
        )
        both_parts = jnp.stack([key_part, value_part], axis=2).reshape(NSEL, BLK, row_width)
        return (grad_table.at[slot_row].add(both_parts), query_part.reshape(QB, heads_here * DH))

    packed = (
        queries.reshape(query_blocks, QB, -1),
        out_grad.reshape(query_blocks, QB, -1),
        log_sums.reshape(query_blocks, QB, -1),
        chosen,
        slot_ids,
        jnp.arange(query_blocks, dtype=jnp.int32),
    )
    start_table = jnp.zeros((key_table.shape[0], BLK, row_width), jnp.float32)
    grad_table, query_parts = lax.scan(one_block, start_table, packed)
    query_grad = query_parts.reshape(tok_count, heads_here * DH)
    returned = lax.all_to_all(
        grad_table.reshape(kv_count, capacity, BLK, row_width),
        "kv",
        split_axis=0,
        concat_axis=0,
        tiled=True,
    )
    targets = jnp.where(asked_ids >= 0, asked_ids, blocks_here).reshape(-1)
    summed = (
        jnp.zeros((blocks_here + 1, BLK, row_width), jnp.float32)
        .at[targets]
        .add(returned.reshape(-1, BLK, row_width))
    )
    kv_grad = summed[:blocks_here].reshape(tok_count, row_width)
    weight_grad = lax.psum_scatter(
        lax.dot_general(
            inputs, query_grad, (((0,), (0,)), ((), ())), preferred_element_type=jnp.float32
        ),
        "kv",
        scatter_dimension=0,
        tiled=True,
    )
    return (query_grad, kv_grad, weight_grad)


def solution(mesh):
    in_specs = (
        P("kv", "tp"),
        P("kv", "tp"),
        P("kv", "tp"),
        P("kv", "tp"),
        P("kv", None),
        P("kv", None),
    )
    out_specs = (P("kv", "tp"), P("kv", "tp"), P("kv", "tp"))
    return jax.shard_map(shards, mesh=mesh, in_specs=in_specs, out_specs=out_specs, check_vma=False)
```

profile of v0, /device:TPU:0, one launch (start us, length us, event | category | flops | bytes accessed | tf_op | source)
XLA Modules:
  0.0 514.7 jit_solution(17658362699768816245)
XLA Ops:
  8.9 13.6 %all_to_all.19 = s32[8,1,6]{2,1,0:T(1,128)S(1)} all-to-all(s32[8,1,6]{2,1,0:T(1,128)S(1)} %copy.64), channel_id=1, replica_groups=mesh['kv'=8,'tp'=4] {'kv'}, dimensions={0} | all-to-all | bytes 384 | tf_op jit(solution)/shard_map/all_to_all | solution.py:40
  25.7 4.3 all-to-all-start.1
  31.5 34.4 %all-to-all-done.1 = bf16[8,6,64,256]{3,2,1,0:T(8,128)(2,1)} async-done(((bf16[8,6,64,256]{3,2,1,0:T(8,128)(2,1)}), bf16[8,6,64,256]{3,2,1,0:T(8,128)(2,1)}, u32[]{:S(2)}, u32[]{:S(2)}) %all-to-all-start.1) | async-done | bytes 1572896 | tf_op jit(solution)/shard_map/all_to_all | solution.py:43
  68.6 216.6 %while.12 = (s32[]{:T(128)}, f32[48,64,256]{2,1,0:T(8,128)}, bf16[6,128,512]{2,1,0:T(8,128)(2,1)}, s32[6,16]{1,0:T(8,128)S(1)}, bf16[6,128,512]{2,1,0:T(8,128)(2...) while((s32[]{:T(128)}, f32[48,64,256]{2,1,0:T(8,128)}, ...), condition=%wide.region_7.8_spmd, body=%wide.region_4.7_spmd.sunk | while | flops 821232896 | bytes 62707756 | solution.py:100
  76.4 3.7 fusion.66
  82.7 3.9 convolution_bitcast_fusion.5
  87.8 3.2 fusion.67
  98.8 3.8 scatter_fusion
  112.6 3.7 fusion.66
  118.9 3.9 convolution_bitcast_fusion.5
  124.1 3.2 fusion.67
  135.1 3.7 scatter_fusion
  148.8 3.7 fusion.66
  155.1 3.9 convolution_bitcast_fusion.5
  160.2 3.2 fusion.67
  171.2 3.7 scatter_fusion
  184.8 3.7 fusion.66
  191.2 3.9 convolution_bitcast_fusion.5
  196.3 3.2 fusion.67
  207.3 3.7 scatter_fusion
  220.9 3.7 fusion.66
  227.3 3.9 convolution_bitcast_fusion.5
  232.4 3.2 fusion.67
  243.4 3.7 scatter_fusion
  257.0 3.7 fusion.66
  263.3 3.9 convolution_bitcast_fusion.5
  279.5 3.6 scatter_fusion
  285.3 9.7 %convolution_bitcast_fusion.3 = f32[4096,512]{0,1:T(8,128)} fusion(bf16[768,512]{1,0:T(8,128)(2,1)} %bitcast.164, bf16[768,4096]{1,0:T(8,128)(2,1)} %param.12), kind=kOutput, calls=%fused_computation.42 | convolution fusion | flops 3221225472 | bytes 15466496 | tf_op jit(solution)/shard_map/dot_general | solution.py:117
  295.0 3.7 all-to-all-start.2
  298.8 136.4 %all-to-all-done.2 = f32[8,6,64,256]{3,2,1,0:T(8,128)S(1)} async-done(((f32[8,6,64,256]{3,2,1,0:T(8,128)}), f32[8,6,64,256]{3,2,1,0:T(8,128)S(1)}, u32[]{:S(2)}, u32[]{:S(2)}) %all-to-all-start.2) | async-done | bytes 3145760 | tf_op jit(solution)/shard_map/all_to_all | solution.py:102
  437.0 6.7 %scatter_fusion.1 = f32[13,64,256]{2,1,0:T(8,128)S(1)} fusion(f32[13,64,256]{2,1,0:T(8,128)S(1)} %broadcast_in_dim.57, s32[48]{0:T(128)S(1)} %fusion.22, f32[48,64,256]{2,1,0:T(8,128)} %bitcast.159), kind=kCustom, calls=%fused_computation.4 | custom fusion | flops 786432 | bytes 9437376 | tf_op jit(solution)/shard_map/scatter-add | solution.py:113
  444.7 60.6 %reduce-scatter.2.cloned.1.call-done = f32[512,512]{0,1:T(8,128)} async-done(((f32[4096,512]{0,1:T(8,128)}), f32[512,512]{0,1:T(8,128)}) %reduce-scatter.2.cloned.1.call-update) | async-done | bytes 1048592 | tf_op jit(solution)/shard_map/reduce_scatter | solution.py:116
  (281 shorter events, 142.7 us)
Async XLA Ops:
  7.2 16.6 %copy-start = (bf16[768,256]{1,0:T(8,128)(2,1)S(1)}, bf16[768,256]{1,0:T(8,128)(2,1)}, u32[]{:S(2)}) copy-start(bf16[768,256]{1,0:T(8,128)(2,1)} %param.9) | copy-start | bytes 1179652
  7.2 22.9 %copy-start.7 = (s32[6,16]{1,0:T(8,128)S(1)}, s32[6,16]{1,0:T(8,128)}, u32[]{:S(2)}) copy-start(s32[6,16]{1,0:T(8,128)} %param.13) | copy-start | bytes 1156
  25.7 40.3 %all-to-all-start.1 = ((bf16[8,6,64,256]{3,2,1,0:T(8,128)(2,1)}), bf16[8,6,64,256]{3,2,1,0:T(8,128)(2,1)}, u32[]{:S(2)}, u32[]{:S(2)}) async-start(bf16[8,6,64,256]{3,2,1,0:T(8,128)(2,1)} %bitcast.32), calls=%async_computation.1 | async-start | bytes 3145728 | tf_op jit(solution)/shard_map/all_to_all | solution.py:43
  30.0 475.3 %reduce-scatter.2.cloned.1.call-start = ((), (), s32[]{:S(2)}) async-start(), calls=%async_computation.4 | async-start | bytes 9437184 | tf_op jit(solution)/shard_map/reduce_scatter | solution.py:116
  75.1 5.7 %copy-start.8 = (s32[6]{0:T(128)S(1)}, s32[6]{0:T(128)}, u32[]{:S(2)}) copy-start(s32[6]{0:T(128)} %get-tuple-element.259) | copy-start | bytes 76 | tf_op jit(solution)/shard_map/while
  75.1 7.6 %copy-start.6 = (bf16[1,128,512]{1,2,0:T(8,128)(2,1)S(1)}, bf16[1,128,512]{1,2,0:T(8,128)(2,1)}, u32[]{:S(2)}) copy-start(bf16[1,128,512]{1,2,0:T(8,128)(2,1)} %copy.96) | copy-start | bytes 393220 | tf_op jit(solution)/shard_map/while
  76.4 10.2 %copy-start.2 = (bf16[1024,2,1,64]{0,3,1,2:T(8,128)(2,1)}, bf16[1024,2,1,64]{0,3,1,2:T(8,128)(2,1)S(1)}, u32[]{:S(2)}) copy-start(bf16[1024,2,1,64]{0,3,1,2:T(8,128)(2,1)S(1)} %copy.98) | copy-start | bytes 786436 | tf_op jit(solution)/shard_map/while
  87.8 3.5 copy-start.1
  111.3 5.7 %copy-start.8 = (s32[6]{0:T(128)S(1)}, s32[6]{0:T(128)}, u32[]{:S(2)}) copy-start(s32[6]{0:T(128)} %get-tuple-element.259) | copy-start | bytes 76 | tf_op jit(solution)/shard_map/while
  111.3 7.6 %copy-start.6 = (bf16[1,128,512]{1,2,0:T(8,128)(2,1)S(1)}, bf16[1,128,512]{1,2,0:T(8,128)(2,1)}, u32[]{:S(2)}) copy-start(bf16[1,128,512]{1,2,0:T(8,128)(2,1)} %copy.96) | copy-start | bytes 393220 | tf_op jit(solution)/shard_map/while
  112.6 10.2 %copy-start.2 = (bf16[1024,2,1,64]{0,3,1,2:T(8,128)(2,1)}, bf16[1024,2,1,64]{0,3,1,2:T(8,128)(2,1)S(1)}, u32[]{:S(2)}) copy-start(bf16[1024,2,1,64]{0,3,1,2:T(8,128)(2,1)S(1)} %copy.98) | copy-start | bytes 786436 | tf_op jit(solution)/shard_map/while
  124.1 3.5 copy-start.1
  147.5 5.7 %copy-start.8 = (s32[6]{0:T(128)S(1)}, s32[6]{0:T(128)}, u32[]{:S(2)}) copy-start(s32[6]{0:T(128)} %get-tuple-element.259) | copy-start | bytes 76 | tf_op jit(solution)/shard_map/while
  147.5 7.6 %copy-start.6 = (bf16[1,128,512]{1,2,0:T(8,128)(2,1)S(1)}, bf16[1,128,512]{1,2,0:T(8,128)(2,1)}, u32[]{:S(2)}) copy-start(bf16[1,128,512]{1,2,0:T(8,128)(2,1)} %copy.96) | copy-start | bytes 393220 | tf_op jit(solution)/shard_map/while
  148.7 10.2 %copy-start.2 = (bf16[1024,2,1,64]{0,3,1,2:T(8,128)(2,1)}, bf16[1024,2,1,64]{0,3,1,2:T(8,128)(2,1)S(1)}, u32[]{:S(2)}) copy-start(bf16[1024,2,1,64]{0,3,1,2:T(8,128)(2,1)S(1)} %copy.98) | copy-start | bytes 786436 | tf_op jit(solution)/shard_map/while
  160.2 3.5 copy-start.1
  183.5 5.7 %copy-start.8 = (s32[6]{0:T(128)S(1)}, s32[6]{0:T(128)}, u32[]{:S(2)}) copy-start(s32[6]{0:T(128)} %get-tuple-element.259) | copy-start | bytes 76 | tf_op jit(solution)/shard_map/while
  183.6 7.6 %copy-start.6 = (bf16[1,128,512]{1,2,0:T(8,128)(2,1)S(1)}, bf16[1,128,512]{1,2,0:T(8,128)(2,1)}, u32[]{:S(2)}) copy-start(bf16[1,128,512]{1,2,0:T(8,128)(2,1)} %copy.96) | copy-start | bytes 393220 | tf_op jit(solution)/shard_map/while
  184.8 10.2 %copy-start.2 = (bf16[1024,2,1,64]{0,3,1,2:T(8,128)(2,1)}, bf16[1024,2,1,64]{0,3,1,2:T(8,128)(2,1)S(1)}, u32[]{:S(2)}) copy-start(bf16[1024,2,1,64]{0,3,1,2:T(8,128)(2,1)S(1)} %copy.98) | copy-start | bytes 786436 | tf_op jit(solution)/shard_map/while
  196.3 3.5 copy-start.1
  199.8 2.2 copy-start.4
  219.6 5.7 %copy-start.8 = (s32[6]{0:T(128)S(1)}, s32[6]{0:T(128)}, u32[]{:S(2)}) copy-start(s32[6]{0:T(128)} %get-tuple-element.259) | copy-start | bytes 76 | tf_op jit(solution)/shard_map/while
  219.6 7.6 %copy-start.6 = (bf16[1,128,512]{1,2,0:T(8,128)(2,1)S(1)}, bf16[1,128,512]{1,2,0:T(8,128)(2,1)}, u32[]{:S(2)}) copy-start(bf16[1,128,512]{1,2,0:T(8,128)(2,1)} %copy.96) | copy-start | bytes 393220 | tf_op jit(solution)/shard_map/while
  220.9 10.2 %copy-start.2 = (bf16[1024,2,1,64]{0,3,1,2:T(8,128)(2,1)}, bf16[1024,2,1,64]{0,3,1,2:T(8,128)(2,1)S(1)}, u32[]{:S(2)}) copy-start(bf16[1024,2,1,64]{0,3,1,2:T(8,128)(2,1)S(1)} %copy.98) | copy-start | bytes 786436 | tf_op jit(solution)/shard_map/while
  232.4 3.5 copy-start.1
  235.9 2.2 copy-start.4
  255.7 5.7 %copy-start.8 = (s32[6]{0:T(128)S(1)}, s32[6]{0:T(128)}, u32[]{:S(2)}) copy-start(s32[6]{0:T(128)} %get-tuple-element.259) | copy-start | bytes 76 | tf_op jit(solution)/shard_map/while
  255.7 7.6 %copy-start.6 = (bf16[1,128,512]{1,2,0:T(8,128)(2,1)S(1)}, bf16[1,128,512]{1,2,0:T(8,128)(2,1)}, u32[]{:S(2)}) copy-start(bf16[1,128,512]{1,2,0:T(8,128)(2,1)} %copy.96) | copy-start | bytes 393220 | tf_op jit(solution)/shard_map/while
  257.0 10.2 %copy-start.2 = (bf16[1024,2,1,64]{0,3,1,2:T(8,128)(2,1)}, bf16[1024,2,1,64]{0,3,1,2:T(8,128)(2,1)S(1)}, u32[]{:S(2)}) copy-start(bf16[1024,2,1,64]{0,3,1,2:T(8,128)(2,1)S(1)} %copy.98) | copy-start | bytes 786436 | tf_op jit(solution)/shard_map/while
  268.5 3.5 copy-start.1
  272.0 2.2 copy-start.4
  295.0 140.1 %all-to-all-start.2 = ((f32[8,6,64,256]{3,2,1,0:T(8,128)}), f32[8,6,64,256]{3,2,1,0:T(8,128)S(1)}, u32[]{:S(2)}, u32[]{:S(2)}) async-start(f32[8,6,64,256]{3,2,1,0:T(8,128)} %bitcast.38), calls=%async_computation.2 | async-start | bytes 6291456 | tf_op jit(solution)/shard_map/all_to_all | solution.py:102
  (10 other events, 16.8 us)
Sparse Core Ops, SparseCore 0:
  295.2 210.0 reduce-scatter.1
where the time goes:
time: 517 us; the launch traced here: 515 us
  waiting for transfers between devices  231 us (45%)
  local copies, waits for them, and re-layouts  113 us (22%)
  matrix products  95.9 us (19%)
  other arithmetic  33.5 us (6%)
  between operations  14.1 us (3%)
  blocking collectives  13.6 us (3%)
  starting transfers between devices  7.99 us (2%)
    all_to_all x1, waiting for transfers between devices, shards(): lax.all_to_all(grad_table.reshape(kv_count, capacity, BLK, row_width), 'k...  136 us
    reduce_scatter x1, waiting for transfers between devices, shards(): lax.psum_scatter(lax.dot_general(inputs, query_grad, (((0,), (0,)), ((),...  60.6 us
    all_to_all x1, waiting for transfers between devices, shards(): lax.all_to_all(fetched, 'kv', split_axis=0, concat_axis=0, tiled=True)  34.4 us
    reshape x12, local copies, waits for them, and re-layouts, one_block(): jnp.stack([key_part, value_part], axis=2).reshape(NSEL, BLK, row_width)  31.5 us
    dot_general x6, matrix products, one_block(): jnp.einsum('qhgn,qhgd->nhd', prob_round, grad_blk, preferred_element_type...  23.3 us
    dynamic_slice x30, local copies, waits for them, and re-layouts, shards(): grad_table, query_parts = lax.scan(one_block, start_table, packed)  22.8 us
    scatter-add x6, other arithmetic, one_block(): grad_table.at[slot_row].add(both_parts)  22.1 us
    dot_general x6, matrix products, one_block(): jnp.einsum('qhgd,nhd->qhgn', query_blk, key_blk, preferred_element_type=j...  22.1 us
  transfers between devices with their start and end apart: 3, of which 3 were waited for; matrix products, arithmetic and copies ran while one was open for 2% of the time, Pallas kernels for 0%

commit v1 on v0

v1 whole, which is shorter than its diff:
```python
import functools

import jax
import jax.numpy as jnp
from jax import lax
from jax.experimental import pallas as pl
from jax.experimental.pallas import tpu as pltpu
from jax.sharding import PartitionSpec as P

DH = 64
BLK = 64
QB = 128
NSEL = 16
CHUNK = 4
SCALE = DH ** (-0.5)


def attend(group_size, slot_ref, chosen_ref, base_ref, tab_ref, w1_ref, w2_ref, ls_ref, dq_ref, g_ref,
           kv_scr, p_scr, dp_scr, a_scr):
    qb = pl.program_id(1)
    lanes = group_size * QB
    rows = CHUNK * BLK

    @pl.when(qb == 0)
    def _():
        g_ref[...] = jnp.zeros_like(g_ref)

    starts = [pl.multiple_of(slot_ref[qb, j] * BLK, BLK) for j in range(NSEL)]
    for j in range(NSEL):
        kv_scr[j * BLK:(j + 1) * BLK, :] = tab_ref[pl.ds(starts[j], BLK), :]
    lane = lax.broadcasted_iota(jnp.int32, (1, lanes), 1)
    qpos = (base_ref[0] + qb) * QB + lax.rem(lane, QB)
    within = lax.broadcasted_iota(jnp.int32, (BLK, lanes), 0)
    sums = ls_ref[0, 0]
    delta = jnp.zeros((1, lanes), jnp.float32)
    for c in range(NSEL // CHUNK):
        kv = kv_scr[c * rows:(c + 1) * rows, :]
        scores = jnp.dot(kv, w1_ref[0, 0, :, :lanes], preferred_element_type=jnp.float32)
        grads = jnp.dot(kv, w1_ref[0, 0, :, lanes:], preferred_element_type=jnp.float32)
        for i in range(CHUNK):
            block = chosen_ref[qb, c * CHUNK + i]
            last = jnp.where(block >= 0, qpos - block * BLK, -1)
            here = slice(i * BLK, (i + 1) * BLK)
            there = slice(c * rows + i * BLK, c * rows + (i + 1) * BLK)
            prob = jnp.where(within <= last, jnp.exp(scores[here] - sums), jnp.float32(0.0))
            rounded = prob.astype(jnp.bfloat16)
            delta += jnp.sum(rounded.astype(jnp.float32) * grads[here], axis=0, keepdims=True)
            p_scr[there, :] = prob
            dp_scr[there, :] = grads[here]
            a_scr[there, lanes:] = rounded
    for c in range(NSEL // CHUNK):
        there = slice(c * rows, (c + 1) * rows)
        a_scr[there, :lanes] = (p_scr[there, :] * (dp_scr[there, :] - delta)).astype(jnp.bfloat16)
        both = jnp.dot(a_scr[there, :], w2_ref[0, 0], preferred_element_type=jnp.float32)
        for i in range(CHUNK):
            at = pl.ds(starts[c * CHUNK + i], BLK)
            g_ref[at, :] = g_ref[at, :] + both[i * BLK:(i + 1) * BLK]
    dq_t = jnp.dot(kv_scr[...].T, a_scr[:, :lanes], preferred_element_type=jnp.float32)[:DH] * SCALE
    stacked = jnp.concatenate([dq_t[:, g * QB:(g + 1) * QB] for g in range(group_size)], axis=0)
    dq_ref[...] = stacked.T.astype(jnp.bfloat16)


def gather_sum(target_ref, part_ref, out_ref):
    out_ref[...] = jnp.zeros_like(out_ref)

    def step(i, carry):
        target = target_ref[i]

        @pl.when(target >= 0)
        def _():
            at = pl.ds(pl.multiple_of(target * BLK, BLK), BLK)
            frm = pl.ds(pl.multiple_of(i * BLK, BLK), BLK)
            out_ref[at, :] = out_ref[at, :] + part_ref[frm, :].astype(jnp.float32)

        return carry

    lax.fori_loop(0, target_ref.shape[0], step, 0)


def shards(queries, keys_values, log_sums, out_grad, inputs, chosen):
    tok_count = queries.shape[0]
    heads_here = queries.shape[1] // DH
    kv_heads = keys_values.shape[1] // (2 * DH)
    group_size = heads_here // kv_heads
    row_width = keys_values.shape[1]
    blocks_here = tok_count // BLK
    query_blocks = tok_count // QB
    kv_count = lax.axis_size("kv")
    first_block = lax.axis_index("kv") * query_blocks
    capacity = blocks_here // 2
    total_blocks = kv_count * blocks_here
    lanes = group_size * QB
    flat_ids = chosen.reshape(-1)
    needed = jnp.any(
        flat_ids[:, None] == jnp.arange(total_blocks, dtype=jnp.int32)[None, :], axis=0
    )
    needed = needed.reshape(kv_count, blocks_here).astype(jnp.int32)
    rank_in = jnp.cumsum(needed, axis=1) - 1
    matches = (needed[:, :, None] == 1) & (
        rank_in[:, :, None] == jnp.arange(capacity, dtype=jnp.int32)[None, None, :]
    )
    request = jnp.sum(
        matches.astype(jnp.int32) * jnp.arange(blocks_here, dtype=jnp.int32)[None, :, None], axis=1
    )
    request = jnp.where(jnp.any(matches, axis=1), request, -1)
    slot_flat = (jnp.arange(kv_count, dtype=jnp.int32)[:, None] * capacity + rank_in).reshape(-1)
    one_hot = chosen[:, :, None] == jnp.arange(total_blocks, dtype=jnp.int32)[None, None, :]
    slot_ids = jnp.sum(jnp.where(one_hot, slot_flat[None, None, :], 0), axis=2)
    asked_ids = lax.all_to_all(request, "kv", split_axis=0, concat_axis=0, tiled=True)
    local_blocks = keys_values.reshape(blocks_here, BLK, row_width)
    fetched = local_blocks[jnp.maximum(asked_ids, 0)]
    key_table = lax.all_to_all(fetched, "kv", split_axis=0, concat_axis=0, tiled=True).reshape(
        kv_count * capacity * BLK, row_width
    )

    def heads_first(rows):
        split = rows.reshape(query_blocks, QB, kv_heads, group_size, DH)
        return split.transpose(0, 2, 3, 1, 4).reshape(query_blocks, kv_heads, lanes, DH)

    query_rows = heads_first(queries * jnp.bfloat16(SCALE))
    grad_rows = heads_first(out_grad)
    pad = ((0, 0), (0, 0), (0, 0))
    w2 = jnp.concatenate(
        [jnp.pad(query_rows, pad + ((0, DH),)), jnp.pad(grad_rows, pad + ((DH, 0),))], axis=2
    )
    w1 = w2.swapaxes(2, 3)
    sums = (
        log_sums.reshape(query_blocks, QB, kv_heads, group_size)
        .transpose(0, 2, 3, 1)
        .reshape(query_blocks, kv_heads, 1, lanes)
    )
    table_rows = kv_count * capacity * BLK
    keys = NSEL * BLK
    query_grad, grad_table = pl.pallas_call(
        functools.partial(attend, group_size),
        grid_spec=pltpu.PrefetchScalarGridSpec(
            num_scalar_prefetch=3,
            grid=(kv_heads, query_blocks),
            in_specs=[
                pl.BlockSpec((table_rows, 2 * DH), lambda h, q, *_: (0, h)),
                pl.BlockSpec((1, 1, 2 * DH, 2 * lanes), lambda h, q, *_: (q, h, 0, 0)),
                pl.BlockSpec((1, 1, 2 * lanes, 2 * DH), lambda h, q, *_: (q, h, 0, 0)),
                pl.BlockSpec((1, 1, 1, lanes), lambda h, q, *_: (q, h, 0, 0)),
            ],
            out_specs=[
                pl.BlockSpec((QB, group_size * DH), lambda h, q, *_: (q, h)),
                pl.BlockSpec((table_rows, 2 * DH), lambda h, q, *_: (0, h)),
            ],
            scratch_shapes=[
                pltpu.VMEM((keys, 2 * DH), jnp.bfloat16),
                pltpu.VMEM((keys, lanes), jnp.float32),
                pltpu.VMEM((keys, lanes), jnp.float32),
                pltpu.VMEM((keys, 2 * lanes), jnp.bfloat16),
            ],
        ),
        out_shape=[
            jax.ShapeDtypeStruct((tok_count, heads_here * DH), jnp.bfloat16),
            jax.ShapeDtypeStruct((table_rows, row_width), jnp.float32),
        ],
        compiler_params=pltpu.CompilerParams(
            dimension_semantics=("arbitrary", "arbitrary"), vmem_limit_bytes=48 * 1024 * 1024
        ),
        cost_estimate=pl.CostEstimate(
            flops=12 * query_blocks * QB * keys * heads_here * DH,
            bytes_accessed=16 * 1024 * 1024,
            transcendentals=query_blocks * QB * keys * heads_here,
        ),
    )(slot_ids, chosen, first_block[None].astype(jnp.int32), key_table, w1, w2, sums)
    weight_part = lax.dot_general(
        inputs, query_grad, (((0,), (0,)), ((), ())), preferred_element_type=jnp.float32
    ).astype(jnp.bfloat16)
    weight_grad = lax.psum_scatter(weight_part, "kv", scatter_dimension=0, tiled=True).astype(
        jnp.float32
    )
    returned = lax.all_to_all(
        grad_table.astype(jnp.bfloat16).reshape(kv_count, capacity * BLK, row_width),
        "kv",
        split_axis=0,
        concat_axis=0,
        tiled=True,
    ).reshape(table_rows, row_width)
    kv_grad = pl.pallas_call(
        gather_sum,
        in_specs=[
            pl.BlockSpec(memory_space=pltpu.SMEM),
            pl.BlockSpec(memory_space=pltpu.VMEM),
        ],
        out_specs=pl.BlockSpec(memory_space=pltpu.VMEM),
        out_shape=jax.ShapeDtypeStruct((tok_count, row_width), jnp.float32),
    )(asked_ids.reshape(-1), returned)
    return (query_grad, kv_grad, weight_grad)


def solution(mesh):
    in_specs = (
        P("kv", "tp"),
        P("kv", "tp"),
        P("kv", "tp"),
        P("kv", "tp"),
        P("kv", None),
        P("kv", None),
    )
    out_specs = (P("kv", "tp"), P("kv", "tp"), P("kv", "tp"))
    return jax.shard_map(shards, mesh=mesh, in_specs=in_specs, out_specs=out_specs, check_vma=False)
```

time: 517 us -> 237 us (0.46)
  waiting for transfers between devices: 231 us -> 124 us
  matrix products: 95.9 us -> 8.44 us
  local copies, waits for them, and re-layouts: 113 us -> 27.9 us
  Pallas kernels: 0 us -> 32.9 us
  other arithmetic: 33.5 us -> 7.5 us
    dot_general x36 -> x0, matrix products: 86.2 us -> none  [the longest x6 23.3 us: one_block(): jnp.einsum('qhgn,qhgd->nhd', prob_round, grad_blk, preferred_element_type...]
    all_to_all x1, waiting for transfers between devices: 136 us -> 70.1 us  [shards(): lax.all_to_all(grad_table.astype(jnp.bfloat16).reshape(kv_count, capacity...]
    pallas_call x0 -> x2, Pallas kernels: none -> 32.9 us  [the longest x1 29.6 us: shards(): pl.pallas_call(functools.partial(attend, group_size), grid_spec=pltpu.Pre...]
    scatter-add x7 -> x0, other arithmetic: 28.9 us -> none  [the longest x6 22.1 us: one_block(): grad_table.at[slot_row].add(both_parts)]
    reshape x18 -> x4, local copies, waits for them, and re-layouts: 33.9 us -> 5.17 us  [the longest x2 4.58 us: heads_first(): split = rows.reshape(query_blocks, QB, kv_heads, group_size, DH)]
    dynamic_slice x30 -> x0, local copies, waits for them, and re-layouts: 22.8 us -> none  [shards(): grad_table, query_parts = lax.scan(one_block, start_table, packed)]
    all_to_all x1, waiting for transfers between devices: 34.4 us -> 13.9 us  [shards(): lax.all_to_all(fetched, 'kv', split_axis=0, concat_axis=0, tiled=True)]
    reduce_scatter x1, waiting for transfers between devices: 60.6 us -> 40.2 us  [shards(): lax.psum_scatter(weight_part, 'kv', scatter_dimension=0, tiled=True)]
  transfers between devices with their start and end apart: 3 -> 3, of which waited for: 3 -> 3; matrix products, arithmetic and copies ran while one was open for 2% -> 10% of each run, Pallas kernels for 0% -> 1%
where the time goes in v1:
time: 237 us; the launch traced here: 236 us
  waiting for transfers between devices  124 us (52%)
  Pallas kernels  32.9 us (14%)
  local copies, waits for them, and re-layouts  27.9 us (12%)
  between operations  14.1 us (6%)
  blocking collectives  13.6 us (6%)
  matrix products  8.44 us (4%)
  other arithmetic  7.5 us (3%)
  starting transfers between devices  7.2 us (3%)
    all_to_all x1, waiting for transfers between devices, shards(): lax.all_to_all(grad_table.astype(jnp.bfloat16).reshape(kv_count, capacity...  70.1 us
    reduce_scatter x1, waiting for transfers between devices, shards(): lax.psum_scatter(weight_part, 'kv', scatter_dimension=0, tiled=True)  40.2 us
    pallas_call x1, Pallas kernels, shards(): pl.pallas_call(functools.partial(attend, group_size), grid_spec=pltpu.Pre...  29.6 us
    all_to_all x1, waiting for transfers between devices, shards(): lax.all_to_all(fetched, 'kv', split_axis=0, concat_axis=0, tiled=True)  13.9 us
    all_to_all x1, blocking collectives, shards(): lax.all_to_all(request, 'kv', split_axis=0, concat_axis=0, tiled=True)  13.6 us
    unnamed x18, local copies, waits for them, and re-layouts  9 us
    dot_general x1, matrix products, shards(): lax.dot_general(inputs, query_grad, (((0,), (0,)), ((), ())), preferred_e...  8.44 us
  transfers between devices with their start and end apart: 3, of which 3 were waited for; matrix products, arithmetic and copies ran while one was open for 10% of the time, Pallas kernels for 1%

profile of v1, /device:TPU:0, one launch (start us, length us, event | category | flops | bytes accessed | tf_op | source)
XLA Modules:
  0.0 235.9 jit_solution(426219408771217337)
XLA Ops:
  7.2 0.8 eq.55
  8.4 0.2 fusion.6
  8.6 0.2 select_reduce_fusion.1
  8.9 13.6 %all_to_all.16 = s32[8,1,6]{2,1,0:T(1,128)S(1)} all-to-all(s32[8,1,6]{2,1,0:T(1,128)S(1)} %copy.30), channel_id=1, replica_groups=mesh['kv'=8,'tp'=4] {'kv'}, dimensions={0} | all-to-all | bytes 384 | tf_op jit(solution)/shard_map/all_to_all | solution.py:109
  22.5 0.5 broadcast.88
  23.0 0.7 fusion.8
  23.8 1.9 gather_fusion
  25.7 3.6 %all-to-all-start.1 = ((bf16[8,6,64,256]{3,2,1,0:T(8,128)(2,1)}), bf16[8,6,64,256]{3,2,1,0:T(8,128)(2,1)S(1)}, u32[]{:S(2)}, u32[]{:S(2)}) async-start(bf16[8,6,64,256]{3,2,1,0:T(8,128)(2,1)} %bitcast.3), calls=%async_computation.1 | async-start | bytes 3145728 | tf_op jit(solution)/shard_map/all_to_all | solution.py:112
  29.4 0.6 copy.35
  30.1 0.3 copy.31
  30.4 1.9 reshape.104
  32.2 2.0 copy.32
  34.2 2.3 copy.33
  36.5 2.7 %reshape.106 = bf16[6,128,2,4,64]{1,0,4,3,2:T(8,128)(2,1)} reshape(bf16[768,512]{0,1:T(8,128)(2,1)} %copy.33) | data formatting | bytes 1572864 | tf_op jit(solution)/shard_map/reshape | solution.py:117
  39.2 2.7 %copy.34 = bf16[6,2,4,128,64]{4,3,2,1,0:T(8,128)(2,1)} copy(bf16[6,2,4,128,64]{3,0,4,2,1:T(8,128)(2,1)} %bitcast.34) | data formatting | bytes 1572864 | tf_op jit(solution)/shard_map/transpose | solution.py:118
  41.9 4.5 %fusion.3 = (bf16[6,2,1024,128]{3,2,1,0:T(8,128)(2,1)}, bf16[6,2,128,1024]{2,3,1,0:T(8,128)(2,1)}) fusion(bf16[6,2,512,64]{3,2,1,0:T(8,128)(2,1)} %bitcast.31, bf16[6,2,512,64]{3,2,1,0:T(8,128)(2,1)S(1)} %bitcast.30), kind=kLoop, calls=%fused_computation.7 | loop fusion | flops 12582912 | bytes 7864320 | tf_op jit(solution)/shard_map/concatenate | solution.py:123
  46.4 4.7 %copy.36.w1_ref = bf16[6,2,128,1024]{3,2,1,0:T(8,128)(2,1)} copy(bf16[6,2,128,1024]{2,3,1,0:T(8,128)(2,1)} %get-tuple-element.22) | data formatting | bytes 6291456 | tf_op jit(solution)/shard_map/transpose | solution.py:126
  51.1 0.2 select_reduce_fusion.slot_ref
  51.3 13.9 %all-to-all-done.1 = bf16[8,6,64,256]{3,2,1,0:T(8,128)(2,1)S(1)} async-done(((bf16[8,6,64,256]{3,2,1,0:T(8,128)(2,1)}), bf16[8,6,64,256]{3,2,1,0:T(8,128)(2,1)S(1)}, u32[]{:S(2)}, u32[]{:S(2)}) %all-to-all-start.1) | async-done | bytes 1572896 | tf_op jit(solution)/shard_map/all_to_all | solution.py:112
  65.2 1.1 copy-done.1
  66.4 1.4 copy-done.2
  67.8 0.7 copy-done.3
  68.5 29.6 %shard_map.85 = (bf16[768,512]{1,0:T(8,128)(2,1)}, f32[3072,256]{1,0:T(8,128)S(1)}) custom-call(s32[6,16]{1,0:T(8,128)S(1)} %select_reduce_fusion.slot_ref, s32[6,16]{1,0:T(8,128)S(1)} %copy-done.4, s32[1]{0:T(128)} %bitcast.base_ref, bf16[3072,256]{1,0:T(8,128)(2,1)S(1)} %bitcast.27, bf16[6,2,128,1024]{3,2,1,0:T(8,128)(2,1)} %copy.36.w1_ref, ...), custom_call_target="tpu_custom_call" | custom-call | flops 4831838208 | bytes 16777216 | tf_op jit(solution)/shard_map/pallas_call | solution.py:134
  98.1 8.4 %fusion.2 = bf16[4096,512]{0,1:T(8,128)(2,1)} fusion(bf16[768,512]{1,0:T(8,128)(2,1)} %get-tuple-element.16, bf16[768,4096]{1,0:T(8,128)(2,1)} %param.10), kind=kOutput, calls=%fused_computation.6 | convolution fusion | flops 3223322624 | bytes 11272192 | tf_op jit(solution)/shard_map/dot_general | solution.py:169
  106.6 1.3 convert_element_type.29
  107.9 3.6 %all-to-all-start.2 = ((bf16[8,384,256]{2,1,0:T(8,128)(2,1)}), bf16[8,384,256]{2,1,0:T(8,128)(2,1)S(1)}, u32[]{:S(2)}, u32[]{:S(2)}) async-start(bf16[8,384,256]{2,1,0:T(8,128)(2,1)} %bitcast.32), calls=%async_computation.2 | async-start | bytes 3145728 | tf_op jit(solution)/shard_map/all_to_all | solution.py:175
  111.5 0.6 reshape.110.target_ref
  112.1 70.1 %all-to-all-done.2 = bf16[8,384,256]{2,1,0:T(8,128)(2,1)S(1)} async-done(((bf16[8,384,256]{2,1,0:T(8,128)(2,1)}), bf16[8,384,256]{2,1,0:T(8,128)(2,1)S(1)}, u32[]{:S(2)}, u32[]{:S(2)}) %all-to-all-start.2) | async-done | bytes 1572896 | tf_op jit(solution)/shard_map/all_to_all | solution.py:175
  182.2 1.2 copy-done.5
  183.3 3.3 %shard_map.86 = f32[768,256]{1,0:T(8,128)} custom-call(s32[48]{0:T(128)} %reshape.110.target_ref, bf16[3072,256]{1,0:T(8,128)(2,1)} %bitcast.29), custom_call_target="tpu_custom_call" | custom-call | tf_op jit(solution)/shard_map/pallas_call | solution.py:182
  186.6 40.2 %reduce-scatter.2.cloned.1.call-done = bf16[512,512]{0,1:T(8,128)(2,1)} async-done(((bf16[4096,512]{0,1:T(8,128)(2,1)}), bf16[512,512]{0,1:T(8,128)(2,1)}) %reduce-scatter.2.cloned.1.call-update) | async-done | bytes 524304 | tf_op jit(solution)/shard_map/reduce_scatter | solution.py:172
  226.8 2.2 copy.37
  (28 shorter events, 0.8 us)
Async XLA Ops:
  7.2 16.6 %copy-start = (bf16[768,256]{1,0:T(8,128)(2,1)S(1)}, bf16[768,256]{1,0:T(8,128)(2,1)}, u32[]{:S(2)}) copy-start(bf16[768,256]{1,0:T(8,128)(2,1)} %param.7) | copy-start | bytes 1179652
  23.8 5.6 %copy-start.7 = (f32[768,8]{0,1:T(8,128)S(1)}, f32[768,8]{0,1:T(8,128)}, u32[]{:S(2)}) copy-start(f32[768,8]{0,1:T(8,128)} %param.8) | copy-start | bytes 73732
  23.8 6.2 %copy-start.6 = (bf16[768,512]{1,0:T(8,128)(2,1)S(1)}, bf16[768,512]{1,0:T(8,128)(2,1)}, u32[]{:S(2)}) copy-start(bf16[768,512]{1,0:T(8,128)(2,1)} %param.6) | copy-start | bytes 2359300
  25.7 39.5 %all-to-all-start.1 = ((bf16[8,6,64,256]{3,2,1,0:T(8,128)(2,1)}), bf16[8,6,64,256]{3,2,1,0:T(8,128)(2,1)S(1)}, u32[]{:S(2)}, u32[]{:S(2)}) async-start(bf16[8,6,64,256]{3,2,1,0:T(8,128)(2,1)} %bitcast.3), calls=%async_computation.1 | async-start | bytes 3145728 | tf_op jit(solution)/shard_map/all_to_all | solution.py:112
  29.3 197.6 %reduce-scatter.2.cloned.1.call-start = ((), (), s32[]{:S(2)}) async-start(), calls=%async_computation.4 | async-start | bytes 4718592 | tf_op jit(solution)/shard_map/reduce_scatter | solution.py:172
  46.4 4.7 %copy-start.4 = (s32[6,16]{1,0:T(8,128)S(1)}, s32[6,16]{1,0:T(8,128)}, u32[]{:S(2)}) copy-start(s32[6,16]{1,0:T(8,128)} %chosen_ref.1) | copy-start | bytes 1156
  65.2 1.1 copy-start.1
  66.4 1.4 copy-start.2
  67.8 0.7 copy-start.3
  107.9 74.2 %all-to-all-start.2 = ((bf16[8,384,256]{2,1,0:T(8,128)(2,1)}), bf16[8,384,256]{2,1,0:T(8,128)(2,1)S(1)}, u32[]{:S(2)}, u32[]{:S(2)}) async-start(bf16[8,384,256]{2,1,0:T(8,128)(2,1)} %bitcast.32), calls=%async_computation.2 | async-start | bytes 3145728 | tf_op jit(solution)/shard_map/all_to_all | solution.py:175
  182.2 1.2 copy-start.5
Sparse Core Ops, SparseCore 0:
  106.7 120.0 reduce-scatter.1

commit v2 on v1

--- a/solution.py
+++ b/solution.py
@@ -7,6 +7,7 @@
 from jax.experimental.pallas import tpu as pltpu
 from jax.sharding import PartitionSpec as P
 
+
 DH = 64
 BLK = 64
 QB = 128
@@ -15,28 +16,33 @@
 SCALE = DH ** (-0.5)
 
 
-def attend(group_size, slot_ref, chosen_ref, base_ref, tab_ref, w1_ref, w2_ref, ls_ref, dq_ref, g_ref,
-           kv_scr, p_scr, dp_scr, a_scr):
-    qb = pl.program_id(1)
+def attend(group_size, parts, slot_ref, chosen_ref, base_ref, *refs):
+    tab_refs, refs = refs[:parts], refs[parts:]
+    w1_ref, w2_ref, ls_ref, dq_ref = refs[:4]
+    g_refs, (tab_scr, g_scr, kv_scr, p_scr, dp_scr, a_scr) = refs[4:4 + parts], refs[4 + parts:]
+    qb = pl.program_id(0)
     lanes = group_size * QB
     rows = CHUNK * BLK
+    span = tab_refs[0].shape[0]
 
     @pl.when(qb == 0)
     def _():
-        g_ref[...] = jnp.zeros_like(g_ref)
+        g_scr[...] = jnp.zeros_like(g_scr)
+        for i in range(parts):
+            tab_scr[i * span:(i + 1) * span, :] = tab_refs[i][...]
 
     starts = [pl.multiple_of(slot_ref[qb, j] * BLK, BLK) for j in range(NSEL)]
     for j in range(NSEL):
-        kv_scr[j * BLK:(j + 1) * BLK, :] = tab_ref[pl.ds(starts[j], BLK), :]
+        kv_scr[j * BLK:(j + 1) * BLK, :] = tab_scr[pl.ds(starts[j], BLK), :]
     lane = lax.broadcasted_iota(jnp.int32, (1, lanes), 1)
     qpos = (base_ref[0] + qb) * QB + lax.rem(lane, QB)
     within = lax.broadcasted_iota(jnp.int32, (BLK, lanes), 0)
-    sums = ls_ref[0, 0]
+    sums = ls_ref[0]
     delta = jnp.zeros((1, lanes), jnp.float32)
     for c in range(NSEL // CHUNK):
         kv = kv_scr[c * rows:(c + 1) * rows, :]
-        scores = jnp.dot(kv, w1_ref[0, 0, :, :lanes], preferred_element_type=jnp.float32)
-        grads = jnp.dot(kv, w1_ref[0, 0, :, lanes:], preferred_element_type=jnp.float32)
+        scores = jnp.dot(kv, w1_ref[0, :, :lanes], preferred_element_type=jnp.float32)
+        grads = jnp.dot(kv, w1_ref[0, :, lanes:], preferred_element_type=jnp.float32)
         for i in range(CHUNK):
             block = chosen_ref[qb, c * CHUNK + i]
             last = jnp.where(block >= 0, qpos - block * BLK, -1)
@@ -51,13 +57,18 @@
     for c in range(NSEL // CHUNK):
         there = slice(c * rows, (c + 1) * rows)
         a_scr[there, :lanes] = (p_scr[there, :] * (dp_scr[there, :] - delta)).astype(jnp.bfloat16)
-        both = jnp.dot(a_scr[there, :], w2_ref[0, 0], preferred_element_type=jnp.float32)
+        both = jnp.dot(a_scr[there, :], w2_ref[0], preferred_element_type=jnp.float32)
         for i in range(CHUNK):
             at = pl.ds(starts[c * CHUNK + i], BLK)
-            g_ref[at, :] = g_ref[at, :] + both[i * BLK:(i + 1) * BLK]
+            g_scr[at, :] = g_scr[at, :] + both[i * BLK:(i + 1) * BLK]
     dq_t = jnp.dot(kv_scr[...].T, a_scr[:, :lanes], preferred_element_type=jnp.float32)[:DH] * SCALE
     stacked = jnp.concatenate([dq_t[:, g * QB:(g + 1) * QB] for g in range(group_size)], axis=0)
     dq_ref[...] = stacked.T.astype(jnp.bfloat16)
+
+    @pl.when(qb == pl.num_programs(0) - 1)
+    def _():
+        for i in range(parts):
+            g_refs[i][...] = g_scr[i * span:(i + 1) * span, :].astype(g_refs[i].dtype)
 
 
 def gather_sum(target_ref, part_ref, out_ref):
@@ -129,51 +140,59 @@
         .transpose(0, 2, 3, 1)
         .reshape(query_blocks, kv_heads, 1, lanes)
     )
-    table_rows = kv_count * capacity * BLK
     keys = NSEL * BLK
-    query_grad, grad_table = pl.pallas_call(
-        functools.partial(attend, group_size),
-        grid_spec=pltpu.PrefetchScalarGridSpec(
-            num_scalar_prefetch=3,
-            grid=(kv_heads, query_blocks),
-            in_specs=[
-                pl.BlockSpec((table_rows, 2 * DH), lambda h, q, *_: (0, h)),
-                pl.BlockSpec((1, 1, 2 * DH, 2 * lanes), lambda h, q, *_: (q, h, 0, 0)),
-                pl.BlockSpec((1, 1, 2 * lanes, 2 * DH), lambda h, q, *_: (q, h, 0, 0)),
-                pl.BlockSpec((1, 1, 1, lanes), lambda h, q, *_: (q, h, 0, 0)),
-            ],
-            out_specs=[
-                pl.BlockSpec((QB, group_size * DH), lambda h, q, *_: (q, h)),
-                pl.BlockSpec((table_rows, 2 * DH), lambda h, q, *_: (0, h)),
-            ],
-            scratch_shapes=[
-                pltpu.VMEM((keys, 2 * DH), jnp.bfloat16),
-                pltpu.VMEM((keys, lanes), jnp.float32),
-                pltpu.VMEM((keys, lanes), jnp.float32),
-                pltpu.VMEM((keys, 2 * lanes), jnp.bfloat16),
-            ],
-        ),
-        out_shape=[
-            jax.ShapeDtypeStruct((tok_count, heads_here * DH), jnp.bfloat16),
-            jax.ShapeDtypeStruct((table_rows, row_width), jnp.float32),
-        ],
-        compiler_params=pltpu.CompilerParams(
-            dimension_semantics=("arbitrary", "arbitrary"), vmem_limit_bytes=48 * 1024 * 1024
-        ),
-        cost_estimate=pl.CostEstimate(
-            flops=12 * query_blocks * QB * keys * heads_here * DH,
-            bytes_accessed=16 * 1024 * 1024,
-            transcendentals=query_blocks * QB * keys * heads_here,
-        ),
-    )(slot_ids, chosen, first_block[None].astype(jnp.int32), key_table, w1, w2, sums)
-    weight_part = lax.dot_general(
-        inputs, query_grad, (((0,), (0,)), ((), ())), preferred_element_type=jnp.float32
-    ).astype(jnp.bfloat16)
-    weight_grad = lax.psum_scatter(weight_part, "kv", scatter_dimension=0, tiled=True).astype(
-        jnp.float32
-    )
-    returned = lax.all_to_all(
-        grad_table.astype(jnp.bfloat16).reshape(kv_count, capacity * BLK, row_width),
+    span = table_rows = kv_count * capacity * BLK
+    base = first_block[None].astype(jnp.int32)
+    query_grads, weight_grads, returned = [], [], []
+    for h in range(kv_heads):
+        attention = pl.pallas_call(
+            functools.partial(attend, group_size, 1),
+            grid_spec=pltpu.PrefetchScalarGridSpec(
+                num_scalar_prefetch=3,
+                grid=(query_blocks,),
+                in_specs=[pl.BlockSpec((span, 2 * DH), lambda q, *_, h=h: (0, h))]
+                + [
+                    pl.BlockSpec((1, None, 2 * DH, 2 * lanes), lambda q, *_, h=h: (q, h, 0, 0)),
+                    pl.BlockSpec((1, None, 2 * lanes, 2 * DH), lambda q, *_, h=h: (q, h, 0, 0)),
+                    pl.BlockSpec((1, None, 1, lanes), lambda q, *_, h=h: (q, h, 0, 0)),
+                ],
+                out_specs=[pl.BlockSpec((QB, group_size * DH), lambda q, *_: (q, 0))]
+                + [pl.BlockSpec((span, 2 * DH), lambda q, *_: (0, 0))],
+                scratch_shapes=[
+                    pltpu.VMEM((span, 2 * DH), jnp.bfloat16),
+                    pltpu.VMEM((span, 2 * DH), jnp.float32),
+                    pltpu.VMEM((keys, 2 * DH), jnp.bfloat16),
+                    pltpu.VMEM((keys, lanes), jnp.float32),
+                    pltpu.VMEM((keys, lanes), jnp.float32),
+                    pltpu.VMEM((keys, 2 * lanes), jnp.bfloat16),
+                ],
+            ),
+            out_shape=[jax.ShapeDtypeStruct((tok_count, group_size * DH), jnp.bfloat16)]
+            + [jax.ShapeDtypeStruct((span, 2 * DH), jnp.bfloat16)],
+            compiler_params=pltpu.CompilerParams(
+                dimension_semantics=("arbitrary",), vmem_limit_bytes=40 * 1024 * 1024
+            ),
+            cost_estimate=pl.CostEstimate(
+                flops=12 * query_blocks * QB * keys * group_size * DH,
+                bytes_accessed=8 * 1024 * 1024,
+                transcendentals=query_blocks * QB * keys * group_size,
+            ),
+        )
+        outs = attention(slot_ids, chosen, base, key_table, w1, w2, sums)
+        query_grads.append(outs[0])
+        returned.append(outs[1])
+        weight_part = lax.dot_general(
+            inputs, outs[0], (((0,), (0,)), ((), ())), preferred_element_type=jnp.float32
+        ).astype(jnp.bfloat16)
+        weight_part, base = lax.optimization_barrier((weight_part, base))
+        weight_grads.append(
+            lax.psum_scatter(weight_part, "kv", scatter_dimension=0, tiled=True)
+        )
+    query_grad = jnp.concatenate(query_grads, axis=1)
+    weight_grad = jnp.concatenate(weight_grads, axis=1).astype(jnp.float32)
+    grad_table = jnp.concatenate(returned, axis=1)
+    received = lax.all_to_all(
+        grad_table.reshape(kv_count, capacity * BLK, row_width),
         "kv",
         split_axis=0,
         concat_axis=0,
@@ -187,7 +206,7 @@
         ],
         out_specs=pl.BlockSpec(memory_space=pltpu.VMEM),
         out_shape=jax.ShapeDtypeStruct((tok_count, row_width), jnp.float32),
-    )(asked_ids.reshape(-1), returned)
+    )(asked_ids.reshape(-1), received)
     return (query_grad, kv_grad, weight_grad)
 
 

time: 237 us -> 254 us (1.072)
  waiting for transfers between devices: 124 us -> 136 us
  matrix products: 8.44 us -> 12.2 us
    reduce_scatter x1 -> x2, waiting for transfers between devices: 40.2 us -> 80 us  [shards(): lax.psum_scatter(weight_part, 'kv', scatter_dimension=0, tiled=True)]
    all_to_all x1, waiting for transfers between devices: 70.1 us -> 35.3 us  [shards(): lax.all_to_all(grad_table.reshape(kv_count, capacity * BLK, row_width), '...]
    all_to_all x1, waiting for transfers between devices: 13.9 us -> 21 us  [shards(): lax.all_to_all(fetched, 'kv', split_axis=0, concat_axis=0, tiled=True)]
    dot_general x1 -> x2, matrix products: 8.44 us -> 12.2 us  [shards(): lax.dot_general(inputs, outs[0], (((0,), (0,)), ((), ())), preferred_elem...]
    unnamed x18 -> x36, local copies, waits for them, and re-layouts: 9 us -> 12.5 us
    pallas_call x1 -> x2, Pallas kernels: 29.6 us -> 30.3 us  [shards(): outs = attention(slot_ids, chosen, base, key_table, w1, w2, sums)]
  transfers between devices with their start and end apart: 3 -> 4, of which waited for: 3 -> 4; matrix products, arithmetic and copies ran while one was open for 10% -> 10% of each run, Pallas kernels for 1% -> 7%
where the time goes in v2:
time: 254 us; the launch traced here: 253 us
  waiting for transfers between devices  136 us (54%)
  Pallas kernels  33.6 us (13%)
  local copies, waits for them, and re-layouts  26.5 us (10%)
  between operations  14.3 us (6%)
  blocking collectives  13.6 us (5%)
  matrix products  12.2 us (5%)
  other arithmetic  8.5 us (3%)
  starting transfers between devices  8.15 us (3%)
    reduce_scatter x2, waiting for transfers between devices, shards(): lax.psum_scatter(weight_part, 'kv', scatter_dimension=0, tiled=True)  80 us
    all_to_all x1, waiting for transfers between devices, shards(): lax.all_to_all(grad_table.reshape(kv_count, capacity * BLK, row_width), '...  35.3 us
    pallas_call x2, Pallas kernels, shards(): outs = attention(slot_ids, chosen, base, key_table, w1, w2, sums)  30.3 us
    all_to_all x1, waiting for transfers between devices, shards(): lax.all_to_all(fetched, 'kv', split_axis=0, concat_axis=0, tiled=True)  21 us
    all_to_all x1, blocking collectives, shards(): lax.all_to_all(request, 'kv', split_axis=0, concat_axis=0, tiled=True)  13.6 us
    unnamed x36, local copies, waits for them, and re-layouts  12.5 us
    dot_general x2, matrix products, shards(): lax.dot_general(inputs, outs[0], (((0,), (0,)), ((), ())), preferred_elem...  12.2 us
  transfers between devices with their start and end apart: 4, of which 4 were waited for; matrix products, arithmetic and copies ran while one was open for 10% of the time, Pallas kernels for 7%

profile of v2, /device:TPU:0, one launch (start us, length us, event | category | flops | bytes accessed | tf_op | source)
XLA Modules:
  0.0 253.1 jit_solution(16579801926844720553)
XLA Ops:
  7.2 0.8 eq.55
  8.9 13.6 %all_to_all.16 = s32[8,1,6]{2,1,0:T(1,128)S(1)} all-to-all(s32[8,1,6]{2,1,0:T(1,128)S(1)} %copy.33), channel_id=1, replica_groups=mesh['kv'=8,'tp'=4] {'kv'}, dimensions={0} | all-to-all | bytes 384 | tf_op jit(solution)/shard_map/all_to_all | solution.py:120
  23.8 1.9 gather_fusion
  25.7 4.3 %all-to-all-start.1 = ((bf16[8,6,64,256]{3,2,1,0:T(8,128)(2,1)}), bf16[8,6,64,256]{3,2,1,0:T(8,128)(2,1)}, u32[]{:S(2)}, u32[]{:S(2)}) async-start(bf16[8,6,64,256]{3,2,1,0:T(8,128)(2,1)} %bitcast.3), calls=%async_computation.1 | async-start | bytes 3145728 | tf_op jit(solution)/shard_map/all_to_all | solution.py:123
  31.2 0.9 reshape.104
  32.1 1.0 copy.35
  33.1 1.4 copy.36
  34.5 1.9 reshape.106
  36.3 2.0 copy.37
  38.3 3.3 %fusion.4 = (bf16[6,2,1024,128]{3,2,1,0:T(8,128)(2,1)}, bf16[6,2,128,1024]{2,3,1,0:T(8,128)(2,1)}) fusion(bf16[6,2,512,64]{3,2,1,0:T(8,128)(2,1)S(1)} %bitcast.36, bf16[6,2,512,64]{3,2,1,0:T(8,128)(2,1)S(1)} %bitcast.35), kind=kLoop, calls=%fused_computation.9 | loop fusion | flops 12582912 | bytes 7864320 | tf_op jit(solution)/shard_map/concatenate | solution.py:134
  41.6 3.2 %copy.39.refs_1_ = bf16[6,2,128,1024]{3,2,1,0:T(8,128)(2,1)S(1)} copy(bf16[6,2,128,1024]{2,3,1,0:T(8,128)(2,1)} %get-tuple-element.32) | data formatting | bytes 6291456 | tf_op jit(solution)/shard_map/transpose | solution.py:137
  45.1 21.0 %all-to-all-done.1 = bf16[8,6,64,256]{3,2,1,0:T(8,128)(2,1)} async-done(((bf16[8,6,64,256]{3,2,1,0:T(8,128)(2,1)}), bf16[8,6,64,256]{3,2,1,0:T(8,128)(2,1)}, u32[]{:S(2)}, u32[]{:S(2)}) %all-to-all-start.1) | async-done | bytes 1572896 | tf_op jit(solution)/shard_map/all_to_all | solution.py:123
  66.1 1.9 copy-done.1
  68.7 15.2 %shard_map.85 = (bf16[768,256]{1,0:T(8,128)(2,1)S(1)}, bf16[3072,128]{1,0:T(8,128)(2,1)S(1)}) custom-call(s32[6,16]{1,0:T(8,128)S(1)} %select_reduce_fusion.slot_ref, s32[6,16]{1,0:T(8,128)S(1)} %copy-done.13, s32[1]{0:T(128)} %bitcast.base_ref, bf16[3072,256]{1,0:T(8,128)(2,1)} %bitcast.4.refs_0_, bf16[6,2,128,1024]{3,2,1,0:T(8,128)(2,1)S(1)} %copy.39.refs_1_, ...), custom_call_target="tpu_custom_call" | custom-call | flops 2415919104 | bytes 8388608 | tf_op jit(solution)/shard_map/pallas_call | solution.py:181
  83.9 0.9 copy-done.7
  84.8 0.8 copy-done.3
  85.5 6.0 %fusion.2 = bf16[4096,256]{0,1:T(8,128)(2,1)} fusion(bf16[768,256]{1,0:T(8,128)(2,1)S(1)} %get-tuple-element.10, bf16[768,4096]{1,0:T(8,128)(2,1)} %param.10), kind=kOutput, calls=%fused_computation.7 | convolution fusion | flops 1611661312 | bytes 8781824 | tf_op jit(solution)/shard_map/dot_general | solution.py:184
  91.7 1.9 copy-done.2
  94.3 15.2 %shard_map.86 = (bf16[768,256]{1,0:T(8,128)(2,1)S(1)}, bf16[3072,128]{1,0:T(8,128)(2,1)S(1)}) custom-call(s32[6,16]{1,0:T(8,128)S(1)} %select_reduce_fusion.slot_ref, s32[6,16]{1,0:T(8,128)S(1)} %copy-done.13, s32[1]{0:T(128)} %bitcast.base_ref, bf16[3072,256]{1,0:T(8,128)(2,1)} %bitcast.4.refs_0_, bf16[6,2,128,1024]{3,2,1,0:T(8,128)(2,1)S(1)} %copy.39.refs_1_, ...), custom_call_target="tpu_custom_call" | custom-call | flops 2415919104 | bytes 8388608 | tf_op jit(solution)/shard_map/pallas_call | solution.py:181
  109.5 0.9 copy-done.9
  110.4 0.7 copy-done.5
  111.2 6.2 %fusion.3 = bf16[4096,256]{0,1:T(8,128)(2,1)} fusion(bf16[768,256]{1,0:T(8,128)(2,1)S(1)} %get-tuple-element.12, bf16[768,4096]{1,0:T(8,128)(2,1)} %param.10), kind=kOutput, calls=%fused_computation.8 | convolution fusion | flops 1611661312 | bytes 8781824 | tf_op jit(solution)/shard_map/dot_general | solution.py:184
  117.4 1.4 pad_maximum_fusion
  118.8 3.6 %all-to-all-start.2 = ((bf16[8,384,256]{2,1,0:T(8,128)(2,1)}), bf16[8,384,256]{2,1,0:T(8,128)(2,1)S(1)}, u32[]{:S(2)}, u32[]{:S(2)}) async-start(bf16[8,384,256]{2,1,0:T(8,128)(2,1)} %bitcast.34), calls=%async_computation.2 | async-start | bytes 3145728 | tf_op jit(solution)/shard_map/all_to_all | solution.py:194
  123.1 0.9 pad_maximum_fusion.1
  124.0 35.3 %all-to-all-done.2 = bf16[8,384,256]{2,1,0:T(8,128)(2,1)S(1)} async-done(((bf16[8,384,256]{2,1,0:T(8,128)(2,1)}), bf16[8,384,256]{2,1,0:T(8,128)(2,1)S(1)}, u32[]{:S(2)}, u32[]{:S(2)}) %all-to-all-start.2) | async-done | bytes 1572896 | tf_op jit(solution)/shard_map/all_to_all | solution.py:194
  159.3 1.2 copy-done.14
  160.6 3.3 %shard_map.87 = f32[768,256]{1,0:T(8,128)} custom-call(s32[48]{0:T(128)} %reshape.110.target_ref, bf16[3072,256]{1,0:T(8,128)(2,1)} %bitcast.33), custom_call_target="tpu_custom_call" | custom-call | tf_op jit(solution)/shard_map/pallas_call | solution.py:201
  163.8 8.6 %reduce-scatter.3.cloned.1.call-done = bf16[512,256]{0,1:T(8,128)(2,1)} async-done(((bf16[4096,256]{0,1:T(8,128)(2,1)}), bf16[512,256]{0,1:T(8,128)(2,1)}) %reduce-scatter.3.cloned.1.call-update) | async-done | bytes 262160 | tf_op jit(solution)/shard_map/reduce_scatter | solution.py:189
  172.4 71.3 %reduce-scatter.5.cloned.1.call-done = bf16[512,256]{0,1:T(8,128)(2,1)} async-done(((bf16[4096,256]{0,1:T(8,128)(2,1)}), bf16[512,256]{0,1:T(8,128)(2,1)}) %reduce-scatter.5.cloned.1.call-update) | async-done | bytes 262160 | tf_op jit(solution)/shard_map/reduce_scatter | solution.py:189
  243.8 1.2 maximum_convert_fusion
  244.9 1.3 copy.41
  (53 shorter events, 5.9 us)
Async XLA Ops:
  7.2 16.6 %copy-start = (bf16[768,256]{1,0:T(8,128)(2,1)S(1)}, bf16[768,256]{1,0:T(8,128)(2,1)}, u32[]{:S(2)}) copy-start(bf16[768,256]{1,0:T(8,128)(2,1)} %param.7) | copy-start | bytes 1179652
  23.8 6.4 %copy-start.16 = (f32[768,8]{0,1:T(8,128)S(1)}, f32[768,8]{0,1:T(8,128)}, u32[]{:S(2)}) copy-start(f32[768,8]{0,1:T(8,128)} %param.8) | copy-start | bytes 73732
  23.8 7.0 %copy-start.15 = (bf16[768,512]{1,0:T(8,128)(2,1)S(1)}, bf16[768,512]{1,0:T(8,128)(2,1)}, u32[]{:S(2)}) copy-start(bf16[768,512]{1,0:T(8,128)(2,1)} %param.6) | copy-start | bytes 2359300
  25.7 40.3 %all-to-all-start.1 = ((bf16[8,6,64,256]{3,2,1,0:T(8,128)(2,1)}), bf16[8,6,64,256]{3,2,1,0:T(8,128)(2,1)}, u32[]{:S(2)}, u32[]{:S(2)}) async-start(bf16[8,6,64,256]{3,2,1,0:T(8,128)(2,1)} %bitcast.3), calls=%async_computation.1 | async-start | bytes 3145728 | tf_op jit(solution)/shard_map/all_to_all | solution.py:123
  30.0 142.4 %reduce-scatter.3.cloned.1.call-start = ((), (), s32[]{:S(2)}) async-start(), calls=%async_computation.5 | async-start | bytes 2359296 | tf_op jit(solution)/shard_map/reduce_scatter | solution.py:189
  41.6 3.2 %copy-start.13 = (s32[6,16]{1,0:T(8,128)S(1)}, s32[6,16]{1,0:T(8,128)}, u32[]{:S(2)}) copy-start(s32[6,16]{1,0:T(8,128)} %chosen_ref.3) | copy-start | bytes 1156
  66.1 1.9 copy-start.1
  67.9 0.7 copy-start.11
  83.9 0.9 copy-start.7
  84.8 0.8 copy-start.3
  91.5 152.3 %reduce-scatter.5.cloned.1.call-start = ((), (), s32[]{:S(2)}) async-start(), calls=%async_computation.6 | async-start | bytes 2359296 | tf_op jit(solution)/shard_map/reduce_scatter | solution.py:189
  91.7 1.9 copy-start.2
  93.6 0.7 copy-start.12
  109.5 0.9 copy-start.9
  110.4 0.7 copy-start.5
  111.2 6.2 %copy-start.8 = (bf16[3072,128]{1,0:T(8,128)(2,1)S(1)}, bf16[3072,128]{1,0:T(8,128)(2,1)}, u32[]{:S(2)}) copy-start(bf16[3072,128]{1,0:T(8,128)(2,1)} %copy-done.7) | copy-start | bytes 2359300
  111.2 6.3 %copy-start.10 = (bf16[3072,128]{1,0:T(8,128)(2,1)S(1)}, bf16[3072,128]{1,0:T(8,128)(2,1)}, u32[]{:S(2)}) copy-start(bf16[3072,128]{1,0:T(8,128)(2,1)} %copy-done.9) | copy-start | bytes 2359300
  117.4 5.6 %copy-start.4 = (bf16[768,256]{1,0:T(8,128)(2,1)S(1)}, bf16[768,256]{1,0:T(8,128)(2,1)}, u32[]{:S(2)}) copy-start(bf16[768,256]{1,0:T(8,128)(2,1)} %copy-done.3) | copy-start | bytes 1179652
  117.4 5.6 %copy-start.6 = (bf16[768,256]{1,0:T(8,128)(2,1)S(1)}, bf16[768,256]{1,0:T(8,128)(2,1)}, u32[]{:S(2)}) copy-start(bf16[768,256]{1,0:T(8,128)(2,1)} %copy-done.5) | copy-start | bytes 1179652
  118.8 40.5 %all-to-all-start.2 = ((bf16[8,384,256]{2,1,0:T(8,128)(2,1)}), bf16[8,384,256]{2,1,0:T(8,128)(2,1)S(1)}, u32[]{:S(2)}, u32[]{:S(2)}) async-start(bf16[8,384,256]{2,1,0:T(8,128)(2,1)} %bitcast.34), calls=%async_computation.2 | async-start | bytes 3145728 | tf_op jit(solution)/shard_map/all_to_all | solution.py:194
  159.3 1.2 copy-start.14
Sparse Core Ops, SparseCore 0:
  91.6 80.7 reduce-scatter.2
  176.0 67.7 reduce-scatter.4
